TPU v7x, 32 devices: a whole 2x2x4 slice. The times are simulated.
32 devices in a mesh: grp: 1, fs: 2 (over x), tp: 16 (over z, y, core).
Axes of the slice: x: 2, y: 2, z: 4, core: 2. Of those that a mesh axis runs over, the one named last changes fastest.
Arguments:
- prompt_rows: bfloat16 [512, 2048], P(('grp', 'fs')), may hold values from -6 to 6
- gain_before: float32 [2048], P('fs'), may hold values from 0.1 to 1.9
- gate_before: float32 [2048, 5632], P('fs', 'tp'), may hold values from -0.125 to 0.125
- up_before: float32 [2048, 5632], P('fs', 'tp'), may hold values from -0.125 to 0.125
- down_before: float32 [5632, 2048], P('fs', 'tp'), may hold values from -0.3125 to 0.3125
- gain_after: float32 [2048], P('fs'), may hold values from 0.1 to 1.9
- gate_after: float32 [2048, 5632], P('fs', 'tp'), may hold values from -0.125 to 0.125
- up_after: float32 [2048, 5632], P('fs', 'tp'), may hold values from -0.125 to 0.125
- down_after: float32 [5632, 2048], P('fs', 'tp'), may hold values from -0.3125 to 0.3125
Outputs:
- mixed_rows: bfloat16 [512, 2048], P(('grp', 'fs'))
- served_gate_before: bfloat16 [2048, 5632], P('grp', 'tp')
- served_up_before: bfloat16 [2048, 5632], P('grp', 'tp')
- served_down_before: bfloat16 [5632, 2048], P(('grp', 'tp'))
- served_gate_after: bfloat16 [2048, 5632], P('grp', 'tp')
- served_up_after: bfloat16 [2048, 5632], P('grp', 'tp')
- served_down_after: bfloat16 [5632, 2048], P(('grp', 'tp'))
All inputs are finite; a program needn't handle non-finite values.
Results may differ from a plain program's by a relative error of at most 0.03.
Values may be sent and summed in bfloat16 or wider, within the bound.
No kernel may reach another device: no remote copies, remote signals or barrier semaphores. Data moves between devices by JAX's collectives and lax.ppermute only.
A program may use at most 64 MiB of HBM per device.

v0:
```python
import jax
import jax.numpy as jnp
from jax import lax
from jax.sharding import PartitionSpec as P

EPS = 1e-06


def serve_weights(gain, gate_w, up_w, down_w):
    gate_half = (gain[:, None] * gate_w).astype(jnp.bfloat16)
    up_half = (gain[:, None] * up_w).astype(jnp.bfloat16)
    down_half = down_w.astype(jnp.bfloat16)
    gate_whole, up_whole = (
        lax.all_gather(gate_half, "fs", axis=0, tiled=True),
        lax.all_gather(up_half, "fs", axis=0, tiled=True),
    )
    tall_block = lax.all_gather(down_half, "fs", axis=0, tiled=True)
    down_whole = lax.all_to_all(tall_block, "tp", split_axis=0, concat_axis=1, tiled=True)
    return (gate_whole, up_whole, down_whole)


def half_step(row_block, gate_w, up_w, down_w):
    values = row_block.astype(jnp.float32)
    normed = (values * lax.rsqrt(jnp.mean(values * values, axis=-1, keepdims=True) + EPS)).astype(
        jnp.bfloat16
    )
    gate_pre = jnp.dot(normed, gate_w, preferred_element_type=jnp.float32)
    up_pre = jnp.dot(normed, up_w, preferred_element_type=jnp.float32)
    hidden = (jax.nn.silu(gate_pre) * up_pre).astype(jnp.bfloat16)
    total = lax.psum(
        jnp.dot(hidden, down_w, preferred_element_type=jnp.float32).astype(jnp.bfloat16), "tp"
    ).astype(jnp.float32)
    return (values + 0.5 * total).astype(jnp.bfloat16)


def body(
    prompt_rows,
    gain_before,
    gate_before,
    up_before,
    down_before,
    gain_after,
    gate_after,
    up_after,
    down_after,
):
    gate_one, up_one, down_one = serve_weights(gain_before, gate_before, up_before, down_before)
    gate_two, up_two, down_two = serve_weights(gain_after, gate_after, up_after, down_after)
    middle = half_step(prompt_rows, gate_one, up_one, down_one)
    mixed = half_step(middle, gate_two, up_two, down_two)
    return (mixed, gate_one, up_one, down_one, gate_two, up_two, down_two)


def solution(mesh):
    placed = (
        P(("grp", "fs"), None),
        P("fs"),
        P("fs", "tp"),
        P("fs", "tp"),
        P("fs", "tp"),
        P("fs"),
        P("fs", "tp"),
        P("fs", "tp"),
        P("fs", "tp"),
    )
    return jax.shard_map(
        body,
        mesh=mesh,
        in_specs=placed,
        out_specs=(
            P(("grp", "fs"), None),
            P("grp", "tp"),
            P("grp", "tp"),
            P(("grp", "tp"), None),
            P("grp", "tp"),
            P("grp", "tp"),
            P(("grp", "tp"), None),
        ),
        check_vma=False,
    )
```

profile of v0, /device:TPU:0, one launch (start us, length us, event | category | flops | bytes accessed | tf_op | source)
XLA Modules:
  0.0 390.6 jit_solution(4047119397556258142)
XLA Ops:
  7.2 2.4 convert_element_type.59
  9.8 2.2 multiply_convert_fusion.3
  12.0 26.6 %all-gather.11.cloned.1.call-done = bf16[5632,128]{1,0:T(8,128)(2,1)} async-done(((bf16[2816,128]{1,0:T(8,128)(2,1)}), bf16[5632,128]{1,0:T(8,128)(2,1)}) %all-gather.11.cloned.1.call-update) | async-done | bytes 1441808 | tf_op jit(solution)/shard_map/all_gather | solution.py:17
  38.6 5.6 %all-to-all-start = ((bf16[16,352,128]{2,1,0:T(8,128)(2,1)}), bf16[16,352,128]{2,1,0:T(8,128)(2,1)S(1)}, u32[]{:S(2)}, u32[]{:S(2)}) async-start(bf16[16,352,128]{2,1,0:T(8,128)(2,1)} %bitcast.21), calls=%async_computation | async-start | bytes 2883584 | tf_op jit(solution)/shard_map/all_to_all | solution.py:18
  44.3 2.4 convert_element_type.68
  47.5 18.9 %all-gather.7.cloned.1.call-done = bf16[2048,352]{0,1:T(8,128)(2,1)} async-done(((bf16[1024,352]{0,1:T(8,128)(2,1)}), bf16[2048,352]{0,1:T(8,128)(2,1)}) %all-gather.7.cloned.1.call-update) | async-done | bytes 1441808 | tf_op jit(solution)/shard_map/all_gather | solution.py:14
  66.4 2.0 fusion.14
  68.5 25.8 %all-gather.17.cloned.1.call-done = bf16[5632,128]{1,0:T(8,128)(2,1)} async-done(((bf16[2816,128]{1,0:T(8,128)(2,1)}), bf16[5632,128]{1,0:T(8,128)(2,1)}) %all-gather.17.cloned.1.call-update) | async-done | bytes 1441808 | tf_op jit(solution)/shard_map/all_gather | solution.py:17
  94.3 5.6 %all-to-all-start.1 = ((bf16[16,352,128]{2,1,0:T(8,128)(2,1)}), bf16[16,352,128]{2,1,0:T(8,128)(2,1)S(1)}, u32[]{:S(2)}, u32[]{:S(2)}) async-start(bf16[16,352,128]{2,1,0:T(8,128)(2,1)} %bitcast.20), calls=%async_computation.1 | async-start | bytes 2883584 | tf_op jit(solution)/shard_map/all_to_all | solution.py:18
  100.0 1.3 copy_bitcast_fusion.1
  101.3 20.7 %all-gather.9.cloned.1.call-done = bf16[2048,352]{0,1:T(8,128)(2,1)} async-done(((bf16[1024,352]{0,1:T(8,128)(2,1)}), bf16[2048,352]{0,1:T(8,128)(2,1)}) %all-gather.9.cloned.1.call-update) | async-done | bytes 1441808 | tf_op jit(solution)/shard_map/all_gather | solution.py:15
  122.0 5.3 %convolution_convert_fusion.1 = bf16[256,2048]{1,0:T(8,128)(2,1)} fusion(bf16[352,2048]{1,0:T(8,128)(2,1)} %copy_bitcast_fusion.1, bf16[2048,352]{0,1:T(8,128)(2,1)} %all-gather.9.cloned.1.call-done, bf16[256,2048]{1,0:T(8,128)(2,1)} %param.9, f32[256]{0:T(256)S(1)} %add_rsqrt_fusion.1, f32[256,352]{0,1:T(8,128)S(1)} %fusion.14), kind=kOutput, calls=%fused_computation.7 | convolution fusion | flops 740835328 | bytes 5342208 | tf_op jit(solution)/shard_map/dot_general | solution.py:31
  127.4 2.8 multiply_convert_fusion.1
  131.1 1.3 copy_bitcast_fusion
  132.4 89.0 %all-reduce.3.cloned.1.call-done = bf16[256,2048]{1,0:T(8,128)(2,1)} async-done(((bf16[256,2048]{1,0:T(8,128)(2,1)}), bf16[256,2048]{1,0:T(8,128)(2,1)}) %all-reduce.3.cloned.1.call-update) | async-done | bytes 1048592 | tf_op jit(solution)/shard_map/psum | solution.py:30
  221.3 1.8 fusion.3
  223.2 25.0 %all-gather.13.cloned.1.call-done = bf16[2048,352]{0,1:T(8,128)(2,1)} async-done(((bf16[1024,352]{0,1:T(8,128)(2,1)}), bf16[2048,352]{0,1:T(8,128)(2,1)}) %all-gather.13.cloned.1.call-update) | async-done | bytes 1441808 | tf_op jit(solution)/shard_map/all_gather | solution.py:14
  248.1 2.1 fusion.10
  250.3 25.7 %all-gather.15.cloned.1.call-done = bf16[2048,352]{0,1:T(8,128)(2,1)} async-done(((bf16[1024,352]{0,1:T(8,128)(2,1)}), bf16[2048,352]{0,1:T(8,128)(2,1)}) %all-gather.15.cloned.1.call-update) | async-done | bytes 1441808 | tf_op jit(solution)/shard_map/all_gather | solution.py:15
  276.0 4.4 %convolution_convert_fusion = bf16[256,2048]{1,0:T(8,128)(2,1)} fusion(bf16[352,2048]{1,0:T(8,128)(2,1)S(1)} %copy-done.9, bf16[2048,352]{0,1:T(8,128)(2,1)} %all-gather.15.cloned.1.call-done, bf16[256,2048]{1,0:T(8,128)(2,1)S(1)} %get-tuple-element.8, f32[256]{0:T(256)S(1)} %add_rsqrt_fusion, f32[256,352]{0,1:T(8,128)S(1)} %fusion.10), kind=kOutput, calls=%fused_computation.6 | convolution fusion | flops 740835328 | bytes 5342208 | tf_op jit(solution)/shard_map/dot_general | solution.py:31
  280.5 94.0 %all-reduce.5.cloned.1.call-done = bf16[256,2048]{1,0:T(8,128)(2,1)} async-done(((bf16[256,2048]{1,0:T(8,128)(2,1)}), bf16[256,2048]{1,0:T(8,128)(2,1)}) %all-reduce.5.cloned.1.call-update) | async-done | bytes 1048592 | tf_op jit(solution)/shard_map/psum | solution.py:30
  374.4 2.6 fusion.5
  377.0 1.1 copy.30
  378.9 1.1 copy.31
  (45 shorter events, 6.5 us)
Async XLA Ops:
  7.2 2.6 copy-start.2
  7.2 2.6 copy-start.3
  7.2 31.4 %all-gather.11.cloned.1.call-start = ((), (), s32[]{:S(2)}) async-start(), calls=%async_computation.4 | async-start | bytes 2162688 | tf_op jit(solution)/shard_map/all_gather | solution.py:17
  9.7 56.7 %all-gather.7.cloned.1.call-start = ((), (), s32[]{:S(2)}) async-start(), calls=%async_computation.2 | async-start | bytes 2162688 | tf_op jit(solution)/shard_map/all_gather | solution.py:14
  38.6 55.7 %all-to-all-start = ((bf16[16,352,128]{2,1,0:T(8,128)(2,1)}), bf16[16,352,128]{2,1,0:T(8,128)(2,1)S(1)}, u32[]{:S(2)}, u32[]{:S(2)}) async-start(bf16[16,352,128]{2,1,0:T(8,128)(2,1)} %bitcast.21), calls=%async_computation | async-start | bytes 2883584 | tf_op jit(solution)/shard_map/all_to_all | solution.py:18
  44.2 3.0 copy-start
  44.2 50.1 %all-gather.17.cloned.1.call-start = ((), (), s32[]{:S(2)}) async-start(), calls=%async_computation.8 | async-start | bytes 2162688 | tf_op jit(solution)/shard_map/all_gather | solution.py:17
  46.7 75.4 %all-gather.9.cloned.1.call-start = ((), (), s32[]{:S(2)}) async-start(), calls=%async_computation.3 | async-start | bytes 2162688 | tf_op jit(solution)/shard_map/all_gather | solution.py:15
  94.3 36.8 %all-to-all-start.1 = ((bf16[16,352,128]{2,1,0:T(8,128)(2,1)}), bf16[16,352,128]{2,1,0:T(8,128)(2,1)S(1)}, u32[]{:S(2)}, u32[]{:S(2)}) async-start(bf16[16,352,128]{2,1,0:T(8,128)(2,1)} %bitcast.20), calls=%async_computation.1 | async-start | bytes 2883584 | tf_op jit(solution)/shard_map/all_to_all | solution.py:18
  99.9 121.4 %all-reduce.3.cloned.1.call-start = ((), (), s32[]{:S(2)}) async-start(), calls=%async_computation.5 | async-start | bytes 2097152 | tf_op jit(solution)/shard_map/psum | solution.py:30
  101.3 26.1 %copy-start.10 = (f32[1024]{0:T(1024)S(1)}, f32[1024]{0:T(1024)}, u32[]{:S(2)}) copy-start(f32[1024]{0:T(1024)} %param.14) | copy-start | bytes 12292
  122.0 5.4 %copy-start.4 = (f32[1024,352]{0,1:T(8,128)S(1)}, f32[1024,352]{0,1:T(8,128)}, u32[]{:S(2)}) copy-start(f32[1024,352]{0,1:T(8,128)} %param.15) | copy-start | bytes 4325380
  127.3 120.8 %all-gather.13.cloned.1.call-start = ((), (), s32[]{:S(2)}) async-start(), calls=%async_computation.6 | async-start | bytes 2162688 | tf_op jit(solution)/shard_map/all_gather | solution.py:14
  130.3 145.7 %all-gather.15.cloned.1.call-start = ((), (), s32[]{:S(2)}) async-start(), calls=%async_computation.7 | async-start | bytes 2162688 | tf_op jit(solution)/shard_map/all_gather | solution.py:15
  131.0 90.3 %copy-start.1 = (bf16[256,2048]{1,0:T(8,128)(2,1)S(1)}, bf16[256,2048]{1,0:T(8,128)(2,1)}, u32[]{:S(2)}) copy-start(bf16[256,2048]{1,0:T(8,128)(2,1)} %param.9) | copy-start | bytes 3145732
  131.0 243.4 %all-reduce.5.cloned.1.call-start = ((), (), s32[]{:S(2)}) async-start(), calls=%async_computation.9 | async-start | bytes 2097152 | tf_op jit(solution)/shard_map/psum | solution.py:30
  248.1 27.9 %copy-start.9 = (bf16[352,2048]{1,0:T(8,128)(2,1)S(1)}, bf16[352,2048]{1,0:T(8,128)(2,1)}, u32[]{:S(2)}) copy-start(bf16[352,2048]{1,0:T(8,128)(2,1)} %copy_bitcast_fusion) | copy-start | bytes 4325380
  280.5 96.6 %copy-start.5 = (bf16[2048,352]{0,1:T(8,128)(2,1)S(1)}, bf16[2048,352]{0,1:T(8,128)(2,1)}, u32[]{:S(2)}) copy-start(bf16[2048,352]{0,1:T(8,128)(2,1)} %all-gather.7.cloned.1.call-done) | copy-start | bytes 4325380
  377.0 1.9 copy-start.6
  378.9 1.9 copy-start.7
  380.8 1.9 copy-start.8
Sparse Core Ops, SparseCore 0:
  10.1 28.4 all-gather.10
  40.7 25.6 all-gather.6
  68.6 25.6 all-gather.16
  96.3 25.6 all-gather.8
  127.5 93.8 all-reduce.2
  223.3 24.7 all-gather.12
  250.3 25.6 all-gather.14
  280.6 93.8 all-reduce.4
where the time goes:
time: 391 us
  waiting for transfers between devices  327 us (84%)
  other arithmetic  14.5 us (4%)
  between operations  14.3 us (4%)
  matrix products  13.9 us (4%)
  starting transfers between devices  11.6 us (3%)
  local copies, waits for them, and re-layouts  9.35 us (2%)
    psum x2, waiting for transfers between devices, half_step(): lax.psum(jnp.dot(hidden, down_w, preferred_element_type=jnp.float32).asty...  183 us
    all_gather x2, waiting for transfers between devices, serve_weights(): tall_block = lax.all_gather(down_half, 'fs', axis=0, tiled=True)  52.5 us
    all_gather x2, waiting for transfers between devices, serve_weights(): lax.all_gather(up_half, 'fs', axis=0, tiled=True)  46.5 us
    all_gather x2, waiting for transfers between devices, serve_weights(): lax.all_gather(gate_half, 'fs', axis=0, tiled=True)  43.9 us
    all_to_all x2, starting transfers between devices, serve_weights(): lax.all_to_all(tall_block, 'tp', split_axis=0, concat_axis=1, tiled=True)  11.2 us
    dot_general x2, matrix products, half_step(): jnp.dot(hidden, down_w, preferred_element_type=jnp.float32)  9.75 us
  transfers between devices with their start and end apart: 10, of which 8 were waited for; matrix products, arithmetic and copies ran while one was open for 5% of the time, Pallas kernels for 0%

commit v1 on v0

--- a/solution.py
+++ b/solution.py
@@ -27,8 +27,11 @@
     gate_pre = jnp.dot(normed, gate_w, preferred_element_type=jnp.float32)
     up_pre = jnp.dot(normed, up_w, preferred_element_type=jnp.float32)
     hidden = (jax.nn.silu(gate_pre) * up_pre).astype(jnp.bfloat16)
-    total = lax.psum(
-        jnp.dot(hidden, down_w, preferred_element_type=jnp.float32).astype(jnp.bfloat16), "tp"
+    total = jnp.sum(
+        lax.all_gather(
+            jnp.dot(hidden, down_w, preferred_element_type=jnp.float32).astype(jnp.bfloat16), "tp"
+        ),
+        axis=0,
     ).astype(jnp.float32)
     return (values + 0.5 * total).astype(jnp.bfloat16)
 

time: 391 us -> 486 us (1.24)
  waiting for transfers between devices: 327 us -> 405 us
  other arithmetic: 14.5 us -> 31.2 us
    all_gather x0 -> x2, waiting for transfers between devices: none -> 226 us  [half_step(): lax.all_gather(jnp.dot(hidden, down_w, preferred_element_type=jnp.float32...]
    psum x2 -> x0, waiting for transfers between devices: 183 us -> none  [half_step(): lax.psum(jnp.dot(hidden, down_w, preferred_element_type=jnp.float32).asty...]
    all_to_all x2, waiting for transfers between devices: 0.01 us -> 48.7 us  [serve_weights(): lax.all_to_all(tall_block, 'tp', split_axis=0, concat_axis=1, tiled=True)]
    reduce_sum x0 -> x2, other arithmetic: none -> 18.7 us  [half_step(): jnp.sum(lax.all_gather(jnp.dot(hidden, down_w, preferred_element_type=jnp...]
    all_gather x2, waiting for transfers between devices: 43.9 us -> 34.5 us  [serve_weights(): lax.all_gather(gate_half, 'fs', axis=0, tiled=True)]
  transfers between devices with their start and end apart: 10 -> 10, of which waited for: 8 -> 10; matrix products, arithmetic and copies ran while one was open for 5% -> 6% of each run, Pallas kernels for 0% -> 0%
where the time goes in v1:
time: 486 us; the launch traced here: 485 us
  waiting for transfers between devices  405 us (83%)
  other arithmetic  31.2 us (6%)
  between operations  14.3 us (3%)
  matrix products  13.4 us (3%)
  starting transfers between devices  11.7 us (2%)
  local copies, waits for them, and re-layouts  9.38 us (2%)
    all_gather x2, waiting for transfers between devices, half_step(): lax.all_gather(jnp.dot(hidden, down_w, preferred_element_type=jnp.float32...  226 us
    all_gather x2, waiting for transfers between devices, serve_weights(): tall_block = lax.all_gather(down_half, 'fs', axis=0, tiled=True)  49.5 us
    all_to_all x2, waiting for transfers between devices, serve_weights(): lax.all_to_all(tall_block, 'tp', split_axis=0, concat_axis=1, tiled=True)  48.7 us
    all_gather x2, waiting for transfers between devices, serve_weights(): lax.all_gather(up_half, 'fs', axis=0, tiled=True)  45 us
    all_gather x2, waiting for transfers between devices, serve_weights(): lax.all_gather(gate_half, 'fs', axis=0, tiled=True)  34.5 us
    reduce_sum x2, other arithmetic, half_step(): jnp.sum(lax.all_gather(jnp.dot(hidden, down_w, preferred_element_type=jnp...  18.7 us
    all_to_all x2, starting transfers between devices, serve_weights(): lax.all_to_all(tall_block, 'tp', split_axis=0, concat_axis=1, tiled=True)  11.4 us
  transfers between devices with their start and end apart: 10, of which 10 were waited for; matrix products, arithmetic and copies ran while one was open for 6% of the time, Pallas kernels for 0%

profile of v1, /device:TPU:0, one launch (start us, length us, event | category | flops | bytes accessed | tf_op | source)
XLA Modules:
  0.0 484.7 jit_solution(3072749329134350362)
XLA Ops:
  7.2 2.4 convert_element_type.63
  9.8 2.2 multiply_convert_fusion.3
  12.0 26.6 %all-gather.15.cloned.1.call-done = bf16[5632,128]{1,0:T(8,128)(2,1)} async-done(((bf16[2816,128]{1,0:T(8,128)(2,1)}), bf16[5632,128]{1,0:T(8,128)(2,1)}) %all-gather.15.cloned.1.call-update) | async-done | bytes 1441808 | tf_op jit(solution)/shard_map/all_gather | solution.py:17
  38.6 5.6 %all-to-all-start = ((bf16[16,352,128]{2,1,0:T(8,128)(2,1)}), bf16[16,352,128]{2,1,0:T(8,128)(2,1)S(1)}, u32[]{:S(2)}, u32[]{:S(2)}) async-start(bf16[16,352,128]{2,1,0:T(8,128)(2,1)} %bitcast.25), calls=%async_computation | async-start | bytes 2883584 | tf_op jit(solution)/shard_map/all_to_all | solution.py:18
  45.0 2.4 convert_element_type.72
  47.8 18.7 %all-gather.11.cloned.1.call-done = bf16[2048,352]{0,1:T(8,128)(2,1)} async-done(((bf16[1024,352]{0,1:T(8,128)(2,1)}), bf16[2048,352]{0,1:T(8,128)(2,1)}) %all-gather.11.cloned.1.call-update) | async-done | bytes 1441808 | tf_op jit(solution)/shard_map/all_gather | solution.py:14
  66.4 2.0 fusion.14
  68.5 5.3 %all-to-all-done = bf16[16,352,128]{2,1,0:T(8,128)(2,1)S(1)} async-done(((bf16[16,352,128]{2,1,0:T(8,128)(2,1)}), bf16[16,352,128]{2,1,0:T(8,128)(2,1)S(1)}, u32[]{:S(2)}, u32[]{:S(2)}) %all-to-all-start) | async-done | bytes 1441824 | tf_op jit(solution)/shard_map/all_to_all | solution.py:18
  73.8 1.3 copy_bitcast_fusion.1
  75.1 19.2 %all-gather.13.cloned.1.call-done = bf16[2048,352]{0,1:T(8,128)(2,1)} async-done(((bf16[1024,352]{0,1:T(8,128)(2,1)}), bf16[2048,352]{0,1:T(8,128)(2,1)}) %all-gather.13.cloned.1.call-update) | async-done | bytes 1441808 | tf_op jit(solution)/shard_map/all_gather | solution.py:15
  94.3 4.9 %convolution_convert_fusion.1 = bf16[256,2048]{1,0:T(8,128)(2,1)} fusion(bf16[352,2048]{1,0:T(8,128)(2,1)} %copy_bitcast_fusion.1, bf16[2048,352]{0,1:T(8,128)(2,1)} %all-gather.13.cloned.1.call-done, bf16[256,2048]{1,0:T(8,128)(2,1)S(1)} %copy-done, f32[256]{0:T(256)S(1)} %add_rsqrt_fusion.1, f32[256,352]{0,1:T(8,128)S(1)} %fusion.14), kind=kOutput, calls=%fused_computation.7 | convolution fusion | flops 740835328 | bytes 5342208 | tf_op jit(solution)/shard_map/dot_general | solution.py:32
  99.2 22.8 %all-gather.21.cloned.1.call-done = bf16[5632,128]{1,0:T(8,128)(2,1)} async-done(((bf16[2816,128]{1,0:T(8,128)(2,1)}), bf16[5632,128]{1,0:T(8,128)(2,1)}) %all-gather.21.cloned.1.call-update) | async-done | bytes 1441808 | tf_op jit(solution)/shard_map/all_gather | solution.py:17
  122.0 5.8 %all-to-all-start.1 = ((bf16[16,352,128]{2,1,0:T(8,128)(2,1)}), bf16[16,352,128]{2,1,0:T(8,128)(2,1)S(1)}, u32[]{:S(2)}, u32[]{:S(2)}) async-start(bf16[16,352,128]{2,1,0:T(8,128)(2,1)} %bitcast.24), calls=%async_computation.1 | async-start | bytes 2883584 | tf_op jit(solution)/shard_map/all_to_all | solution.py:18
  127.8 3.3 multiply_convert_fusion.1
  131.9 43.4 %all-to-all-done.1 = bf16[16,352,128]{2,1,0:T(8,128)(2,1)S(1)} async-done(((bf16[16,352,128]{2,1,0:T(8,128)(2,1)}), bf16[16,352,128]{2,1,0:T(8,128)(2,1)S(1)}, u32[]{:S(2)}, u32[]{:S(2)}) %all-to-all-start.1) | async-done | bytes 1441824 | tf_op jit(solution)/shard_map/all_to_all | solution.py:18
  176.6 99.0 %all-gather.23.cloned.1.call-done = bf16[4096,2048]{1,0:T(8,128)(2,1)} async-done(((bf16[256,2048]{1,0:T(8,128)(2,1)}), bf16[4096,2048]{1,0:T(8,128)(2,1)}) %all-gather.23.cloned.1.call-update) | async-done | bytes 16777232 | tf_op jit(solution)/shard_map/all_gather | solution.py:31
  275.7 9.5 %reduce_sum.43 = bf16[256,2048]{1,0:T(8,128)(2,1)S(1)} reduce(bf16[16,256,2048]{2,1,0:T(8,128)(2,1)} %bitcast.22, bf16[]{:T(256)} %constant.15.clone.1), dimensions={0}, to_apply=%region_1.2 | reduce | flops 7864320 | bytes 17825794 | tf_op jit(solution)/shard_map/reduce_sum | solution.py:30
  285.7 15.8 %all-gather.17.cloned.1.call-done = bf16[2048,352]{0,1:T(8,128)(2,1)} async-done(((bf16[1024,352]{0,1:T(8,128)(2,1)}), bf16[2048,352]{0,1:T(8,128)(2,1)}) %all-gather.17.cloned.1.call-update) | async-done | bytes 1441808 | tf_op jit(solution)/shard_map/all_gather | solution.py:14
  301.5 2.1 fusion.10
  303.7 25.7 %all-gather.19.cloned.1.call-done = bf16[2048,352]{0,1:T(8,128)(2,1)} async-done(((bf16[1024,352]{0,1:T(8,128)(2,1)}), bf16[2048,352]{0,1:T(8,128)(2,1)}) %all-gather.19.cloned.1.call-update) | async-done | bytes 1441808 | tf_op jit(solution)/shard_map/all_gather | solution.py:15
  329.4 4.4 convolution_convert_fusion
  333.9 126.6 %all-gather.25.cloned.1.call-done = bf16[4096,2048]{1,0:T(8,128)(2,1)} async-done(((bf16[256,2048]{1,0:T(8,128)(2,1)}), bf16[4096,2048]{1,0:T(8,128)(2,1)}) %all-gather.25.cloned.1.call-update) | async-done | bytes 16777232 | tf_op jit(solution)/shard_map/all_gather | solution.py:31
  460.5 9.3 %reduce_sum.45 = bf16[256,2048]{1,0:T(8,128)(2,1)S(1)} reduce(bf16[16,256,2048]{2,1,0:T(8,128)(2,1)} %bitcast.23, bf16[]{:T(256)} %constant.15.clone.1), dimensions={0}, to_apply=%region_3.4 | reduce | flops 7864320 | bytes 17825794 | tf_op jit(solution)/shard_map/reduce_sum | solution.py:30
  469.7 1.4 fusion.5
  (43 shorter events, 10.8 us)
Async XLA Ops:
  7.2 2.6 copy-start.2
  7.2 2.6 copy-start.1
  7.2 31.4 %all-gather.15.cloned.1.call-start = ((), (), s32[]{:S(2)}) async-start(), calls=%async_computation.4 | async-start | bytes 2162688 | tf_op jit(solution)/shard_map/all_gather | solution.py:17
  9.7 56.7 %all-gather.11.cloned.1.call-start = ((), (), s32[]{:S(2)}) async-start(), calls=%async_computation.2 | async-start | bytes 2162688 | tf_op jit(solution)/shard_map/all_gather | solution.py:14
  38.6 35.2 %all-to-all-start = ((bf16[16,352,128]{2,1,0:T(8,128)(2,1)}), bf16[16,352,128]{2,1,0:T(8,128)(2,1)S(1)}, u32[]{:S(2)}, u32[]{:S(2)}) async-start(bf16[16,352,128]{2,1,0:T(8,128)(2,1)} %bitcast.25), calls=%async_computation | async-start | bytes 2883584 | tf_op jit(solution)/shard_map/all_to_all | solution.py:18
  44.2 50.1 %all-gather.13.cloned.1.call-start = ((), (), s32[]{:S(2)}) async-start(), calls=%async_computation.3 | async-start | bytes 2162688 | tf_op jit(solution)/shard_map/all_gather | solution.py:15
  44.9 2.5 copy-start
  45.0 77.1 %all-gather.21.cloned.1.call-start = ((), (), s32[]{:S(2)}) async-start(), calls=%async_computation.7 | async-start | bytes 2162688 | tf_op jit(solution)/shard_map/all_gather | solution.py:17
  47.4 228.3 %all-gather.23.cloned.1.call-start = ((), (), s32[]{:S(2)}) async-start(), calls=%async_computation.8 | async-start | bytes 17825792 | tf_op jit(solution)/shard_map/all_gather | solution.py:31
  122.0 5.8 %copy-start.8 = (f32[1024]{0:T(1024)S(1)}, f32[1024]{0:T(1024)}, u32[]{:S(2)}) copy-start(f32[1024]{0:T(1024)} %param.14) | copy-start | bytes 12292
  122.0 53.3 %all-to-all-start.1 = ((bf16[16,352,128]{2,1,0:T(8,128)(2,1)}), bf16[16,352,128]{2,1,0:T(8,128)(2,1)S(1)}, u32[]{:S(2)}, u32[]{:S(2)}) async-start(bf16[16,352,128]{2,1,0:T(8,128)(2,1)} %bitcast.24), calls=%async_computation.1 | async-start | bytes 2883584 | tf_op jit(solution)/shard_map/all_to_all | solution.py:18
  127.8 173.8 %all-gather.17.cloned.1.call-start = ((), (), s32[]{:S(2)}) async-start(), calls=%async_computation.5 | async-start | bytes 2162688 | tf_op jit(solution)/shard_map/all_gather | solution.py:14
  131.1 198.3 %all-gather.19.cloned.1.call-start = ((), (), s32[]{:S(2)}) async-start(), calls=%async_computation.6 | async-start | bytes 2162688 | tf_op jit(solution)/shard_map/all_gather | solution.py:15
  131.9 328.6 %all-gather.25.cloned.1.call-start = ((), (), s32[]{:S(2)}) async-start(), calls=%async_computation.9 | async-start | bytes 17825792 | tf_op jit(solution)/shard_map/all_gather | solution.py:31
  301.5 27.9 %copy-start.7 = (bf16[352,2048]{1,0:T(8,128)(2,1)S(1)}, bf16[352,2048]{1,0:T(8,128)(2,1)}, u32[]{:S(2)}) copy-start(bf16[352,2048]{1,0:T(8,128)(2,1)} %copy_bitcast_fusion) | copy-start | bytes 4325380
  469.7 1.4 copy-start.3
  471.1 1.9 copy-start.4
  473.0 1.9 copy-start.5
  474.9 1.9 copy-start.6
Sparse Core Ops, SparseCore 0:
  10.1 28.4 all-gather.14
  40.7 25.6 all-gather.10
  68.6 25.6 all-gather.12
  96.3 25.7 all-gather.20
  124.6 151.0 all-gather.22
  277.6 23.8 all-gather.16
  303.7 25.6 all-gather.18
  334.0 126.4 all-gather.24
